TPU v7x, 128 devices: a whole 4x4x4 slice. The times are simulated.
128 devices in a mesh: sp: 16 (over z, y), tp: 8 (over x, core).
Axes of the slice: x: 4, y: 4, z: 4, core: 2. Of those that a mesh axis runs over, the one named last changes fastest.
Arguments:
- tokens: bfloat16 [12288, 2048], P(('sp', 'tp')), may hold values from -6 to 6
- norm_gain: float32 [2048], replicated, may hold values from 0.1 to 1.9
- w_query: bfloat16 [2048, 1024], P('sp', 'tp'), may hold values from -0.125 to 0.125
- w_forget: bfloat16 [2048, 1024], P('sp', 'tp'), may hold values from -0.125 to 0.125
- w_input: bfloat16 [2048, 1024], P('sp', 'tp'), may hold values from -0.125 to 0.125
- w_outgate: bfloat16 [2048, 1024], P('sp', 'tp'), may hold values from -0.125 to 0.125
- w_conv_value: bfloat16 [2048, 1024], P('sp', 'tp'), may hold values from -0.125 to 0.125
- w_conv_gate: bfloat16 [2048, 1024], P('sp', 'tp'), may hold values from -0.125 to 0.125
- w_gate_rec: bfloat16 [2048, 2048], P('sp', 'tp'), may hold values from -0.125 to 0.125
- w_gate_conv: bfloat16 [2048, 2048], P('sp', 'tp'), may hold values from -0.125 to 0.125
- lower_bound: float32 [1024], P('tp'), may hold values from 0.92 to 0.9999593, as said below
- decay_shift: float32 [12288, 1024], P('sp', 'tp'), may hold values from -0.7 to 0, as said below
- state_init: float32 [8, 128, 128], P('tp'), may hold values from -0.125 to 0.125
- head_gain: float32 [1024], P('tp'), may hold values from 0.1 to 1.9
- conv_kernel: float32 [31, 1024], P(None, 'tp'), may hold values from -7.5 to 7.5
- channel_gain: float32 [1024], P('tp'), may hold values from 0.1 to 1.9
- channel_bias: float32 [1024], P('tp'), may hold values from -3 to 3
- w_out_rec: bfloat16 [1024, 2048], P('tp', 'sp'), may hold values from -0.1875 to 0.1875
- w_out_conv: bfloat16 [1024, 2048], P('tp', 'sp'), may hold values from -0.1875 to 0.1875
Outputs:
- mixed_out: bfloat16 [12288, 2048], P('sp', 'tp')
Inputs may be any that keep to these rules, and one draw needn't show every extreme that they name: `lower_bound`: every entry is below one. `decay_shift`: no entry is positive.
All inputs are finite; a program needn't handle non-finite values.
Results may differ from a plain program's by a relative error of at most 0.017.
Values may be sent and summed in bfloat16 or wider, within the bound.
A program may use at most 64 MiB of HBM per device.

v0:
```python
import jax
import jax.numpy as jnp
from jax import lax
from jax.sharding import PartitionSpec as P

HEAD = 128
CONV = 1024
KW = 31
BLOCK = 64
EPSILON = 1e-06


def in_one_piece(arrays, axis, dim, along):
    ends, at = ([], 0)
    for a in arrays[:-1]:
        at += a.shape[along]
        ends.append(at)
    both = jnp.concatenate(arrays, axis=along)
    return tuple(jnp.split(lax.all_gather(both, axis, axis=dim, tiled=True), ends, axis=along))


def sent_to_all(array, axis):
    size = lax.axis_size(axis)
    return lax.all_to_all(
        jnp.broadcast_to(array[None], (size, *array.shape)), axis, 0, 0, tiled=True
    )


def all_in_one(array, axis):
    leaves = jax.tree.leaves(array)
    sequence = sorted(range(len(leaves)), key=lambda k: -leaves[k].size)
    width = (1, *leaves[sequence[0]].shape)[-1]
    lines = [
        jnp.pad(leaves[k].reshape(-1), (0, -leaves[k].size % width)).reshape(-1, width)
        for k in sequence
    ]
    both, at, found = (sent_to_all(jnp.concatenate(lines), axis), 0, {})
    for k, line in zip(sequence, lines):
        section = both[:, at : at + len(line)].reshape(len(both), -1)
        found[k] = section[:, : leaves[k].size].reshape(-1, *leaves[k].shape)
        at += len(line)
    numbers = iter(range(len(leaves)))
    return jax.tree.map(lambda _: found[next(numbers)], array)


def joined_by_halves(pieces, combine):
    while len(jax.tree.leaves(pieces)[0]) > 1:
        pieces = jax.vmap(combine)(
            *(jax.tree.map(lambda part: part[side::2], pieces) for side in (0, 1))
        )
    return jax.tree.map(lambda part: part[0], pieces)


def entering(array, axis, combine, identity):
    size, position = (lax.axis_size(axis), lax.axis_index(axis))
    passed = jnp.arange(size) < position

    def kept(part, zero, own):
        part = jnp.where(
            passed.reshape(-1, *(1 for _ in own.shape)),
            part.astype(own.dtype),
            jnp.asarray(zero, own.dtype),
        )
        return part

    pieces = all_in_one(
        jax.tree.map(lambda part, kind: part.astype(kind), array, (jnp.bfloat16, jnp.bfloat16)),
        axis,
    )
    return joined_by_halves(jax.tree.map(kept, pieces, identity, array), combine)


def passed_along(block, axis, distance):
    devices = range(lax.axis_size(axis))
    route = [(i - distance, i) for i in devices if i - distance in devices]
    return lax.ppermute(block, axis, route)


def of_everyone(array, axis):
    everything = sent_to_all(array, axis)
    return jnp.sum(everything, axis=0)


def normalize_rows(values, gain_vector):
    widened = values.astype(jnp.float32)
    scale = lax.rsqrt(jnp.mean(widened * widened, axis=-1, keepdims=True) + EPSILON)
    return (widened * scale * gain_vector).astype(jnp.bfloat16)


def block_step(state, inputs):
    query, input_gate, values, log_decay = inputs
    length = query.shape[1]
    causal_masked = (jnp.arange(length)[:, None] >= jnp.arange(length)[None, :])[None, :, :, None]
    cumulative = jnp.cumsum(log_decay, axis=1)
    spread = cumulative[:, :, None, :] - cumulative[:, None, :, :]
    weight = jnp.where(causal_masked, jnp.exp(jnp.where(causal_masked, spread, 0.0)), 0.0)
    scores = jnp.einsum("htd,hsd,htsd->hts", query, input_gate, weight)
    output = jnp.einsum("hts,hsv->htv", scores, values)
    output = output + jnp.einsum("htd,hdv->htv", query * jnp.exp(cumulative), state)
    final = cumulative[:, -1:, :]
    carried = jnp.exp(final[:, 0, :])[:, :, None] * state
    carried = carried + jnp.einsum("hsd,hsv->hdv", input_gate * jnp.exp(final - cumulative), values)
    return (carried, output)


def compose(preceding_segment, later):
    return (preceding_segment[0] * later[0], later[0][..., None] * preceding_segment[1] + later[1])


def local(
    tokens,
    norm_gain,
    w_query,
    w_forget,
    w_input,
    w_outgate,
    w_conv_value,
    w_conv_gate,
    w_gate_rec,
    w_gate_conv,
    lower_bound,
    decay_shift,
    state_init,
    head_gain,
    conv_kernel,
    channel_gain,
    channel_bias,
    w_out_rec,
    w_out_conv,
):
    tp_count = lax.axis_size("tp")
    normed = normalize_rows(lax.all_gather(tokens, "tp", axis=0, tiled=True), norm_gain)
    row_count = normed.shape[0]
    weights = (
        w_query,
        w_forget,
        w_input,
        w_outgate,
        w_conv_value,
        w_conv_gate,
        w_gate_rec,
        w_gate_conv,
    )
    portions = in_one_piece(
        (
            weights[0],
            weights[1],
            weights[2],
            weights[3],
            weights[4],
            weights[5],
            weights[6],
            weights[7],
        ),
        "sp",
        0,
        1,
    )
    sums = tuple(
        (jnp.dot(normed, portion, preferred_element_type=jnp.float32) for portion in portions)
    )
    (
        query_raw,
        forget_raw,
        input_raw,
        outgate_raw,
        value_raw,
        gate_raw,
        gate_rec_raw,
        gate_conv_raw,
    ) = tuple((overall_aggregate.astype(jnp.bfloat16) for overall_aggregate in sums))
    local_heads = w_query.shape[1] // HEAD
    block_count = row_count // BLOCK
    query = jax.nn.silu(query_raw.astype(jnp.float32))
    input_gate = (1.0 - lower_bound) * jax.nn.sigmoid(-forget_raw.astype(jnp.float32))
    log_decay = jnp.log1p(-input_gate) + decay_shift
    values = input_raw.astype(jnp.float32)

    def to_blocks(array):
        return array.reshape(block_count, BLOCK, local_heads, HEAD).transpose(0, 2, 1, 3)

    zero_state = jnp.zeros((local_heads, HEAD, HEAD), jnp.float32)
    local_state, blocks_out = lax.scan(
        block_step,
        zero_state,
        (to_blocks(query), to_blocks(input_gate), to_blocks(values), to_blocks(log_decay)),
    )
    local_out = blocks_out.transpose(0, 2, 1, 3).reshape(row_count, local_heads, HEAD)
    running = jnp.cumsum(log_decay, axis=0)
    cumulated_forgetting = jnp.exp(running[-1]).reshape(local_heads, HEAD)
    ones_decay = jnp.ones_like(cumulated_forgetting)
    prefix_decay, prefix_state = entering(
        (cumulated_forgetting, local_state), "sp", compose, (ones_decay, zero_state)
    )
    incoming_state = prefix_decay[:, :, None] * state_init + prefix_state
    decayed_query = (query * jnp.exp(running)).reshape(row_count, local_heads, HEAD)
    head_out = local_out + jnp.einsum("thd,hdv->thv", decayed_query, incoming_state)
    head_out = head_out * lax.rsqrt(jnp.mean(head_out * head_out, axis=-1, keepdims=True) + EPSILON)
    head_out = head_out * head_gain.reshape(local_heads, HEAD)
    mixed_rec = (
        head_out.reshape(row_count, local_heads * HEAD)
        * jax.nn.silu(outgate_raw.astype(jnp.float32))
    ).astype(jnp.bfloat16)
    gated = (value_raw.astype(jnp.float32) * jax.nn.sigmoid(gate_raw.astype(jnp.float32))).astype(
        jnp.bfloat16
    )
    rim_width = KW - 1
    previous = passed_along(gated[row_count - rim_width :], "sp", 1)
    extended = jnp.concatenate([previous, gated], axis=0).astype(jnp.float32)
    conv_out = jnp.zeros((row_count, gated.shape[1]), jnp.float32)
    for tap_index in range(KW):
        conv_out = conv_out + conv_kernel[tap_index] * extended[tap_index : tap_index + row_count]
    squares = of_everyone(jnp.sum(conv_out * conv_out, axis=1), "tp")
    scale = lax.rsqrt(squares / CONV + EPSILON)[:, None]
    mixed_conv = jax.nn.silu(conv_out * scale * channel_gain + channel_bias).astype(jnp.bfloat16)
    rec_columns, conv_columns = in_one_piece((w_out_rec, w_out_conv), "sp", 1, 0)
    rec_width = mixed_rec.shape[1]
    rec_whole, conv_whole = in_one_piece((rec_columns, conv_columns), "tp", 0, 1)
    both = jnp.concatenate([mixed_rec, mixed_conv], axis=1).reshape(
        tp_count, row_count // tp_count, -1
    )
    arrived = lax.all_to_all(both, "tp", split_axis=0, concat_axis=2, tiled=True)
    item_count = arrived.shape[1]
    grouped = arrived.reshape(item_count, tp_count, -1)
    rec_part = grouped[:, :, :rec_width].reshape(item_count, -1)
    conv_part = grouped[:, :, rec_width:].reshape(item_count, -1)
    first = jnp.dot(rec_part, rec_whole, preferred_element_type=jnp.float32).astype(jnp.bfloat16)
    second = jnp.dot(conv_part, conv_whole, preferred_element_type=jnp.float32).astype(jnp.bfloat16)
    projected = jnp.stack([first, second], axis=1)[None]
    returned = lax.all_to_all(projected[0], "tp", split_axis=2, concat_axis=0, tiled=True)
    y_rec = returned[:, 0]
    y_conv = returned[:, 1]
    merged = jax.nn.sigmoid(gate_rec_raw.astype(jnp.float32)) * y_rec.astype(jnp.float32)
    merged = merged + jax.nn.sigmoid(gate_conv_raw.astype(jnp.float32)) * y_conv.astype(jnp.float32)
    return merged.astype(jnp.bfloat16)


def solution(mesh):
    in_specs = (
        P(("sp", "tp"), None),
        P(),
        P("sp", "tp"),
        P("sp", "tp"),
        P("sp", "tp"),
        P("sp", "tp"),
        P("sp", "tp"),
        P("sp", "tp"),
        P("sp", "tp"),
        P("sp", "tp"),
        P("tp"),
        P("sp", "tp"),
        P("tp", None, None),
        P("tp"),
        P(None, "tp"),
        P("tp"),
        P("tp"),
        P("tp", "sp"),
        P("tp", "sp"),
    )
    out_specs = P("sp", "tp")
    return jax.shard_map(local, mesh=mesh, in_specs=in_specs, out_specs=out_specs, check_vma=False)
```

profile of v0, /device:TPU:1, one launch (start us, length us, event | category | flops | bytes accessed | tf_op | source)
XLA Modules:
  0.0 333.0 jit_solution(5961914956780123622)
XLA Ops:
  16.6 1.6 slice_bitcast_fusion.35
  18.1 1.7 slice_bitcast_fusion.36
  19.8 34.6 %all-gather.9.cloned.1.call-done = bf16[256,2048]{1,0:T(8,128)(2,1)} async-done(((bf16[256,128]{1,0:T(8,128)(2,1)}), bf16[256,2048]{1,0:T(8,128)(2,1)}) %all-gather.9.cloned.1.call-update) | async-done | bytes 1048592 | tf_op jit(solution)/shard_map/all_gather | solution.py:19
  56.8 28.2 %all-gather.5.cloned.1.call-done = bf16[768,2048]{1,0:T(8,128)(2,1)} async-done(((bf16[96,2048]{1,0:T(8,128)(2,1)}), bf16[768,2048]{1,0:T(8,128)(2,1)}) %all-gather.5.cloned.1.call-update) | async-done | bytes 3145744 | tf_op jit(solution)/shard_map/all_gather | solution.py:132
  85.0 2.7 fusion.28
  88.6 54.3 %all-gather.7.cloned.1.call-done = bf16[2048,1280]{1,0:T(8,128)(2,1)} async-done(((bf16[128,1280]{1,0:T(8,128)(2,1)}), bf16[2048,1280]{1,0:T(8,128)(2,1)}) %all-gather.7.cloned.1.call-update) | async-done | bytes 5242896 | tf_op jit(solution)/shard_map/all_gather | solution.py:19
  142.9 2.8 divide_multiply_fusion
  145.7 2.1 convolution_convert_fusion.6
  147.7 2.9 log-plus-one_add_fusion
  150.7 80.2 %while.13 = (s32[]{:T(128)}, f32[1,128,128]{2,1,0:T(8,128)S(1)}, f32[12,1,64,128]{3,2,1,0:T(8,128)}, f32[12,1,64,128]{3,2,1,0:T(8,128)}, f32[12,1,64,128]{3,2,1,...) while((s32[]{:T(128)}, f32[1,128,128]{2,1,0:T(8,128)S(1)}, ...), condition=%wide.region_3.4_spmd.clone, body=%wide.region_1.3_spmd.clone.sunk | while | flops 9003011 | bytes 5051520 | solution.py:183
  153.0 1.7 fusion.167
  154.9 1.5 fusion.169
  159.7 1.7 fusion.167
  161.5 1.5 fusion.169
  166.3 1.7 fusion.167
  168.2 1.5 fusion.169
  173.0 1.7 fusion.167
  174.9 1.5 fusion.169
  179.7 1.7 fusion.167
  181.6 1.5 fusion.169
  186.4 1.7 fusion.167
  193.1 1.7 fusion.167
  199.8 1.7 fusion.167
  206.4 1.7 fusion.167
  208.3 1.5 fusion.169
  213.1 1.7 fusion.167
  215.0 1.5 fusion.169
  219.8 1.7 fusion.167
  221.7 1.5 fusion.169
  226.5 1.7 fusion.167
  228.4 1.5 fusion.169
  234.1 2.2 fusion.69
  236.5 2.0 fusion.68
  238.6 3.1 collective-permute-start
  245.3 5.5 %all-to-all-start.1 = ((f32[8,1,768]{2,1,0:T(1,128)}), f32[8,1,768]{2,1,0:T(1,128)}, u32[]{:S(2)}, u32[]{:S(2)}) async-start(f32[8,1,768]{2,1,0:T(1,128)} %broadcast_in_dim.89), calls=%async_computation.1 | async-start | bytes 49152 | tf_op jit(solution)/shard_map/all_to_all | solution.py:24
  252.2 3.4 %all-to-all-done.1 = f32[8,1,768]{2,1,0:T(1,128)} async-done(((f32[8,1,768]{2,1,0:T(1,128)}), f32[8,1,768]{2,1,0:T(1,128)}, u32[]{:S(2)}, u32[]{:S(2)}) %all-to-all-start.1) | async-done | bytes 24608 | tf_op jit(solution)/shard_map/all_to_all | solution.py:24
  255.6 1.6 broadcast_in_dim.85
  257.3 7.0 %all-to-all-start = ((bf16[16,129,128]{2,1,0:T(8,128)(2,1)}), bf16[16,129,128]{2,1,0:T(8,128)(2,1)}, u32[]{:S(2)}, u32[]{:S(2)}) async-start(bf16[16,129,128]{2,1,0:T(8,128)(2,1)} %broadcast_in_dim.85), calls=%async_computation | async-start | bytes 1114112 | tf_op jit(solution)/shard_map/all_to_all | solution.py:24
  265.1 1.5 multiply_convert_fusion
  266.6 8.4 %all-to-all-done = bf16[16,129,128]{2,1,0:T(8,128)(2,1)} async-done(((bf16[16,129,128]{2,1,0:T(8,128)(2,1)}), bf16[16,129,128]{2,1,0:T(8,128)(2,1)}, u32[]{:S(2)}, u32[]{:S(2)}) %all-to-all-start) | async-done | bytes 528416 | tf_op jit(solution)/shard_map/all_to_all | solution.py:24
  278.2 2.1 fusion.117
  280.3 12.6 %all_to_all.44 = bf16[8,96,256]{2,1,0:T(8,128)(2,1)S(1)} all-to-all(bf16[8,96,256]{2,1,0:T(8,128)(2,1)S(1)} %bitcast.263), channel_id=1, replica_groups=mesh['sp'=16,'tp'=8] {'tp'}, dimensions={0} | all-to-all | bytes 786432 | tf_op jit(solution)/shard_map/all_to_all | solution.py:222
  293.0 3.0 fusion.44
  296.0 3.0 fusion.41
  299.8 18.2 %all_to_all.45 = bf16[96,2,2048]{0,1,2:T(2,128)(2,1)S(1)} all-to-all(bf16[96,2,2048]{0,1,2:T(2,128)(2,1)S(1)} %copy.78), channel_id=1, replica_groups=mesh['sp'=16,'tp'=8] {'tp'}, dimensions={2} | all-to-all | bytes 1572864 | tf_op jit(solution)/shard_map/all_to_all | solution.py:230
  318.1 1.9 copy.79
  320.0 3.4 %fusion.60 = f32[768,256]{1,0:T(8,128)S(1)} fusion(bf16[768,2048]{1,0:T(8,128)(2,1)} %copy-done.1, bf16[2048,1280]{1,0:T(8,128)(2,1)} %all-gather.7.cloned.1.call-done, bf16[768,2,256]{2,0,1:T(8,128)(2,1)} %bitcast.268), kind=kOutput, calls=%fused_computation.65 | convolution fusion | flops 806682624 | bytes 5373952 | tf_op jit(solution)/shard_map/dot_general | solution.py:160
  323.5 3.0 fusion.54
  (251 shorter events, 71.7 us)
Async XLA Ops:
  6.5 47.8 %all-gather.9.cloned.1.call-start = ((), (), s32[]{:S(2)}) async-start(), calls=%async_computation.6 | async-start | bytes 1114112 | tf_op jit(solution)/shard_map/all_gather | solution.py:19
  8.0 77.0 %all-gather.5.cloned.1.call-start = ((), (), s32[]{:S(2)}) async-start(), calls=%async_computation.4 | async-start | bytes 3538944 | tf_op jit(solution)/shard_map/all_gather | solution.py:132
  8.7 134.1 %all-gather.7.cloned.1.call-start = ((), (), s32[]{:S(2)}) async-start(), calls=%async_computation.5 | async-start | bytes 5570560 | tf_op jit(solution)/shard_map/all_gather | solution.py:19
  15.8 277.2 %all-gather.11.cloned.1.call-start = ((), (), s32[]{:S(2)}) async-start(), calls=%async_computation.7 | async-start | bytes 9437184 | tf_op jit(solution)/shard_map/all_gather | solution.py:19
  55.7 32.0 %copy-start.12 = (f32[2048]{0:T(1024)S(1)}, f32[2048]{0:T(1024)}, u32[]{:S(2)}) copy-start(f32[2048]{0:T(1024)} %param.22) | copy-start | bytes 24580
  85.0 2.8 copy-start
  88.6 189.6 %copy-start.1 = (bf16[768,2048]{1,0:T(8,128)(2,1)}, bf16[768,2048]{1,0:T(8,128)(2,1)S(1)}, u32[]{:S(2)}) copy-start(bf16[768,2048]{1,0:T(8,128)(2,1)S(1)} %fusion.30) | copy-start | bytes 9437188
  145.7 2.1 copy-start.40
  232.1 0.8 copy-start.3
  234.1 8.2 %copy-start.4 = (f32[128,6,128]{0,2,1:T(8,128)}, f32[128,6,128]{0,2,1:T(8,128)S(1)}, u32[]{:S(2)}) copy-start(f32[128,6,128]{0,2,1:T(8,128)S(1)} %copy.72) | copy-start | bytes 1179652
  236.3 6.6 %copy-start.13 = (f32[128]{0:T(128)S(1)}, f32[128]{0:T(128)}, u32[]{:S(2)}) copy-start(f32[128]{0:T(128)} %get-tuple-element.149) | copy-start | bytes 1540
  236.3 6.6 %copy-start.14 = (f32[128]{0:T(128)S(1)}, f32[128]{0:T(128)}, u32[]{:S(2)}) copy-start(f32[128]{0:T(128)} %get-tuple-element.150) | copy-start | bytes 1540
  236.3 6.6 %copy-start.15 = (f32[128]{0:T(128)S(1)}, f32[128]{0:T(128)}, u32[]{:S(2)}) copy-start(f32[128]{0:T(128)} %get-tuple-element.151) | copy-start | bytes 1540
  236.3 6.6 %copy-start.16 = (f32[128]{0:T(128)S(1)}, f32[128]{0:T(128)}, u32[]{:S(2)}) copy-start(f32[128]{0:T(128)} %get-tuple-element.152) | copy-start | bytes 1540
  236.3 6.6 %copy-start.17 = (f32[128]{0:T(128)S(1)}, f32[128]{0:T(128)}, u32[]{:S(2)}) copy-start(f32[128]{0:T(128)} %get-tuple-element.153) | copy-start | bytes 1540
  236.3 6.6 %copy-start.18 = (f32[128]{0:T(128)S(1)}, f32[128]{0:T(128)}, u32[]{:S(2)}) copy-start(f32[128]{0:T(128)} %get-tuple-element.154) | copy-start | bytes 1540
  236.3 6.6 %copy-start.19 = (f32[128]{0:T(128)S(1)}, f32[128]{0:T(128)}, u32[]{:S(2)}) copy-start(f32[128]{0:T(128)} %get-tuple-element.155) | copy-start | bytes 1540
  236.3 6.6 %copy-start.20 = (f32[128]{0:T(128)S(1)}, f32[128]{0:T(128)}, u32[]{:S(2)}) copy-start(f32[128]{0:T(128)} %get-tuple-element.156) | copy-start | bytes 1540
  236.4 6.6 %copy-start.21 = (f32[128]{0:T(128)S(1)}, f32[128]{0:T(128)}, u32[]{:S(2)}) copy-start(f32[128]{0:T(128)} %get-tuple-element.126) | copy-start | bytes 1540
  236.4 6.6 %copy-start.22 = (f32[128]{0:T(128)S(1)}, f32[128]{0:T(128)}, u32[]{:S(2)}) copy-start(f32[128]{0:T(128)} %get-tuple-element.127) | copy-start | bytes 1540
  236.4 6.6 %copy-start.23 = (f32[128]{0:T(128)S(1)}, f32[128]{0:T(128)}, u32[]{:S(2)}) copy-start(f32[128]{0:T(128)} %get-tuple-element.128) | copy-start | bytes 1540
  236.4 6.6 %copy-start.24 = (f32[128]{0:T(128)S(1)}, f32[128]{0:T(128)}, u32[]{:S(2)}) copy-start(f32[128]{0:T(128)} %get-tuple-element.129) | copy-start | bytes 1540
  236.4 6.6 %copy-start.25 = (f32[128]{0:T(128)S(1)}, f32[128]{0:T(128)}, u32[]{:S(2)}) copy-start(f32[128]{0:T(128)} %get-tuple-element.130) | copy-start | bytes 1540
  236.4 6.6 %copy-start.26 = (f32[128]{0:T(128)S(1)}, f32[128]{0:T(128)}, u32[]{:S(2)}) copy-start(f32[128]{0:T(128)} %get-tuple-element.131) | copy-start | bytes 1540
  236.4 6.6 %copy-start.27 = (f32[128]{0:T(128)S(1)}, f32[128]{0:T(128)}, u32[]{:S(2)}) copy-start(f32[128]{0:T(128)} %get-tuple-element.132) | copy-start | bytes 1540
  236.4 6.6 %copy-start.28 = (f32[128]{0:T(128)S(1)}, f32[128]{0:T(128)}, u32[]{:S(2)}) copy-start(f32[128]{0:T(128)} %get-tuple-element.133) | copy-start | bytes 1540
  236.4 6.6 %copy-start.29 = (f32[128]{0:T(128)S(1)}, f32[128]{0:T(128)}, u32[]{:S(2)}) copy-start(f32[128]{0:T(128)} %get-tuple-element.134) | copy-start | bytes 1540
  236.4 6.6 %copy-start.30 = (f32[128]{0:T(128)S(1)}, f32[128]{0:T(128)}, u32[]{:S(2)}) copy-start(f32[128]{0:T(128)} %get-tuple-element.135) | copy-start | bytes 1540
  236.5 6.6 %copy-start.31 = (f32[128]{0:T(128)S(1)}, f32[128]{0:T(128)}, u32[]{:S(2)}) copy-start(f32[128]{0:T(128)} %get-tuple-element.136) | copy-start | bytes 1540
  236.5 6.6 %copy-start.32 = (f32[128]{0:T(128)S(1)}, f32[128]{0:T(128)}, u32[]{:S(2)}) copy-start(f32[128]{0:T(128)} %get-tuple-element.137) | copy-start | bytes 1540
  236.5 6.6 %copy-start.33 = (f32[128]{0:T(128)S(1)}, f32[128]{0:T(128)}, u32[]{:S(2)}) copy-start(f32[128]{0:T(128)} %get-tuple-element.138) | copy-start | bytes 1540
  236.5 6.6 %copy-start.34 = (f32[128]{0:T(128)S(1)}, f32[128]{0:T(128)}, u32[]{:S(2)}) copy-start(f32[128]{0:T(128)} %get-tuple-element.139) | copy-start | bytes 1540
  236.5 6.6 %copy-start.35 = (f32[128]{0:T(128)S(1)}, f32[128]{0:T(128)}, u32[]{:S(2)}) copy-start(f32[128]{0:T(128)} %get-tuple-element.140) | copy-start | bytes 1540
  236.5 6.6 %copy-start.36 = (f32[128]{0:T(128)S(1)}, f32[128]{0:T(128)}, u32[]{:S(2)}) copy-start(f32[128]{0:T(128)} %get-tuple-element.141) | copy-start | bytes 1540
  236.5 6.6 %copy-start.37 = (f32[128]{0:T(128)S(1)}, f32[128]{0:T(128)}, u32[]{:S(2)}) copy-start(f32[128]{0:T(128)} %get-tuple-element.142) | copy-start | bytes 1540
  236.5 6.6 %copy-start.38 = (f32[128]{0:T(128)S(1)}, f32[128]{0:T(128)}, u32[]{:S(2)}) copy-start(f32[128]{0:T(128)} %get-tuple-element.143) | copy-start | bytes 1540
  236.5 6.6 %copy-start.39 = (f32[128]{0:T(128)S(1)}, f32[128]{0:T(128)}, u32[]{:S(2)}) copy-start(f32[128]{0:T(128)} %get-tuple-element.144) | copy-start | bytes 1540
  238.6 4.3 %collective-permute-start = (bf16[30,128]{1,0:T(8,128)(2,1)S(1)}, bf16[30,128]{1,0:T(8,128)(2,1)S(1)}, u32[]{:S(2)}, u32[]{:S(2)}) collective-permute-start(bf16[30,128]{1,0:T(8,128)(2,1)S(1)} %slice.369), channel_id=1, source_target_pairs={{0,8},{8,16},{16,24},{24,32},{32,40},{40,48},{48,56},{56,64},{64,7... | collective-permute-start | bytes 23048 | tf_op jit(solution)/shard_map/ppermute | solution.py:76
  245.3 10.3 %all-to-all-start.1 = ((f32[8,1,768]{2,1,0:T(1,128)}), f32[8,1,768]{2,1,0:T(1,128)}, u32[]{:S(2)}, u32[]{:S(2)}) async-start(f32[8,1,768]{2,1,0:T(1,128)} %broadcast_in_dim.89), calls=%async_computation.1 | async-start | bytes 49152 | tf_op jit(solution)/shard_map/all_to_all | solution.py:24
  257.3 17.8 %all-to-all-start = ((bf16[16,129,128]{2,1,0:T(8,128)(2,1)}), bf16[16,129,128]{2,1,0:T(8,128)(2,1)}, u32[]{:S(2)}, u32[]{:S(2)}) async-start(bf16[16,129,128]{2,1,0:T(8,128)(2,1)} %broadcast_in_dim.85), calls=%async_computation | async-start | bytes 1114112 | tf_op jit(solution)/shard_map/all_to_all | solution.py:24
  266.6 11.1 %copy-start.5 = (f32[128,6,128]{0,2,1:T(8,128)S(1)}, f32[128,6,128]{0,2,1:T(8,128)}, u32[]{:S(2)}) copy-start(f32[128,6,128]{0,2,1:T(8,128)} %copy-done.4) | copy-start | bytes 1179652
  266.6 11.5 %copy-start.41 = (f32[128]{0:T(128)S(1)}, f32[128]{0:T(128)}, u32[]{:S(2)}) copy-start(f32[128]{0:T(128)} %param.34) | copy-start | bytes 1540
  275.1 2.6 copy-start.6
  275.1 2.6 copy-start.10
  275.1 2.7 copy-start.11
  278.2 2.1 copy-start.8
  320.0 3.4 %copy-start.2 = (bf16[768,2048]{1,0:T(8,128)(2,1)S(1)}, bf16[768,2048]{1,0:T(8,128)(2,1)}, u32[]{:S(2)}) copy-start(bf16[768,2048]{1,0:T(8,128)(2,1)} %copy-done.1) | copy-start | bytes 9437188
  320.0 3.5 %copy-start.7 = (bf16[96,2,8,256]{3,0,2,1:T(8,128)(2,1)S(1)}, bf16[96,2,8,256]{3,0,2,1:T(8,128)(2,1)}, u32[]{:S(2)}) copy-start(bf16[96,2,8,256]{3,0,2,1:T(8,128)(2,1)} %copy.79) | copy-start | bytes 2359300
  (1 other events, 0.7 us)
Sparse Core Ops, SparseCore 0:
  9.4 44.8 all-gather.8
  56.0 28.8 all-gather.4
  87.1 55.7 all-gather.6
  144.4 49.7 all-gather.10
where the time goes:
time: 338 us; the launch traced here: 333 us
  waiting for transfers between devices  130 us (38%)
  matrix products  58.7 us (17%)
  other arithmetic  47.2 us (14%)
  local copies, waits for them, and re-layouts  36.5 us (11%)
  blocking collectives  30.8 us (9%)
  starting transfers between devices  15.8 us (5%)
  between operations  13.9 us (4%)
    all_gather x3, waiting for transfers between devices, in_one_piece(): lax.all_gather(both, axis, axis=dim, tiled=True)  88.9 us
    all_gather x1, waiting for transfers between devices, local(): lax.all_gather(tokens, 'tp', axis=0, tiled=True)  28.2 us
    dot_general x12, other arithmetic, block_step(): scores = jnp.einsum('htd,hsd,htsd->hts', query, input_gate, weight)  20.5 us
    dot_general x8, matrix products, local(): jnp.dot(normed, portion, preferred_element_type=jnp.float32)  20.5 us
    all_to_all x1, blocking collectives, local(): lax.all_to_all(projected[0], 'tp', split_axis=2, concat_axis=0, tiled=True)  18.2 us
    dot_general x12, matrix products, block_step(): jnp.einsum('htd,hdv->htv', query * jnp.exp(cumulative), state)  18.2 us
    all_to_all x2, starting transfers between devices, sent_to_all(): lax.all_to_all(jnp.broadcast_to(array[None], (size, *array.shape)), axis,...  12.6 us
    all_to_all x1, blocking collectives, local(): lax.all_to_all(both, 'tp', split_axis=0, concat_axis=2, tiled=True)  12.6 us
  transfers between devices with their start and end apart: 7, of which 5 were waited for; matrix products, arithmetic and copies ran while one was open for 37% of the time, Pallas kernels for 0%

commit v1 on v0

--- a/solution.py
+++ b/solution.py
@@ -1,3 +1,4 @@
+import functools
 import jax
 import jax.numpy as jnp
 from jax import lax
@@ -8,6 +9,14 @@
 KW = 31
 BLOCK = 64
 EPSILON = 1e-06
+
+
+def hold_orders(mine, dim_no):
+    b_now = jnp.concatenate(lax.axis_size("tp") * [mine], axis=dim_no)
+    return lax.all_to_all(b_now, "tp", dim_no, dim_no, tiled=True)
+
+
+_match_ranges = functools.partial(hold_orders, dim_no=0)
 
 
 def in_one_piece(arrays, axis, dim, along):
@@ -129,7 +138,7 @@
     w_out_conv,
 ):
     tp_count = lax.axis_size("tp")
-    normed = normalize_rows(lax.all_gather(tokens, "tp", axis=0, tiled=True), norm_gain)
+    normed = normalize_rows(_match_ranges(tokens), norm_gain)
     row_count = normed.shape[0]
     weights = (
         w_query,

time: 338 us -> 310 us (0.917)
  waiting for transfers between devices: 130 us -> 92.6 us
  starting transfers between devices: 15.8 us -> 21.6 us
    all_gather x1 -> x0, waiting for transfers between devices: 28.2 us -> none  [local(): lax.all_gather(tokens, 'tp', axis=0, tiled=True)]
    all_gather x3, waiting for transfers between devices: 88.9 us -> 74.2 us  [in_one_piece(): lax.all_gather(both, axis, axis=dim, tiled=True)]
    all_to_all x0 -> x1, waiting for transfers between devices: none -> 6.52 us  [hold_orders(): return lax.all_to_all(b_now, 'tp', dim_no, dim_no, tiled=True)]
    all_to_all x0 -> x1, starting transfers between devices: none -> 5.92 us  [hold_orders(): return lax.all_to_all(b_now, 'tp', dim_no, dim_no, tiled=True)]
    unnamed x92 -> x105, local copies, waits for them, and re-layouts: 7.34 us -> 12 us
  transfers between devices with their start and end apart: 7 -> 7, of which waited for: 5 -> 5; matrix products, arithmetic and copies ran while one was open for 37% -> 41% of each run, Pallas kernels for 0% -> 0%
where the time goes in v1:
time: 310 us; the launch traced here: 305 us
  waiting for transfers between devices  92.6 us (30%)
  matrix products  59.7 us (19%)
  other arithmetic  46.2 us (15%)
  local copies, waits for them, and re-layouts  39.4 us (13%)
  blocking collectives  30.8 us (10%)
  starting transfers between devices  21.6 us (7%)
  between operations  13.9 us (4%)
    all_gather x3, waiting for transfers between devices, in_one_piece(): lax.all_gather(both, axis, axis=dim, tiled=True)  74.2 us
    dot_general x8, matrix products, local(): jnp.dot(normed, portion, preferred_element_type=jnp.float32)  21.4 us
    dot_general x12, other arithmetic, block_step(): scores = jnp.einsum('htd,hsd,htsd->hts', query, input_gate, weight)  20.5 us
    all_to_all x1, blocking collectives, local(): lax.all_to_all(projected[0], 'tp', split_axis=2, concat_axis=0, tiled=True)  18.2 us
    dot_general x12, matrix products, block_step(): jnp.einsum('htd,hdv->htv', query * jnp.exp(cumulative), state)  18.2 us
    all_to_all x2, starting transfers between devices, sent_to_all(): lax.all_to_all(jnp.broadcast_to(array[None], (size, *array.shape)), axis,...  12.6 us
    all_to_all x1, blocking collectives, local(): lax.all_to_all(both, 'tp', split_axis=0, concat_axis=2, tiled=True)  12.5 us
    unnamed x105, local copies, waits for them, and re-layouts  12 us
  transfers between devices with their start and end apart: 7, of which 5 were waited for; matrix products, arithmetic and copies ran while one was open for 41% of the time, Pallas kernels for 0%

profile of v1, /device:TPU:1, one launch (start us, length us, event | category | flops | bytes accessed | tf_op | source)
XLA Modules:
  0.0 304.6 jit_solution(1731135993575298035)
XLA Ops:
  18.4 1.6 copy-done.1
  20.0 5.9 %all-to-all-start = ((bf16[8,96,2048]{2,1,0:T(8,128)(2,1)}), bf16[8,96,2048]{2,1,0:T(8,128)(2,1)S(1)}, u32[]{:S(2)}, u32[]{:S(2)}) async-start(bf16[8,96,2048]{2,1,0:T(8,128)(2,1)} %bitcast.267), calls=%async_computation | async-start | bytes 6291456 | tf_op jit(solution)/shard_map/all_to_all | solution.py:16
  27.2 27.2 %all-gather.6.cloned.1.call-done = bf16[256,2048]{1,0:T(8,128)(2,1)} async-done(((bf16[256,128]{1,0:T(8,128)(2,1)}), bf16[256,2048]{1,0:T(8,128)(2,1)}) %all-gather.6.cloned.1.call-update) | async-done | bytes 1048592 | tf_op jit(solution)/shard_map/all_gather | solution.py:28
  56.9 6.5 %all-to-all-done = bf16[8,96,2048]{2,1,0:T(8,128)(2,1)S(1)} async-done(((bf16[8,96,2048]{2,1,0:T(8,128)(2,1)}), bf16[8,96,2048]{2,1,0:T(8,128)(2,1)S(1)}, u32[]{:S(2)}, u32[]{:S(2)}) %all-to-all-start) | async-done | bytes 3145760 | tf_op jit(solution)/shard_map/all_to_all | solution.py:16
  64.2 2.4 fusion.29
  66.6 47.0 %all-gather.4.cloned.1.call-done = bf16[2048,1280]{1,0:T(8,128)(2,1)} async-done(((bf16[128,1280]{1,0:T(8,128)(2,1)}), bf16[2048,1280]{1,0:T(8,128)(2,1)}) %all-gather.4.cloned.1.call-update) | async-done | bytes 5242896 | tf_op jit(solution)/shard_map/all_gather | solution.py:28
  113.5 3.7 %divide_multiply_fusion = f32[768,128]{1,0:T(8,128)} fusion(bf16[768,2048]{1,0:T(8,128)(2,1)} %fusion.29, bf16[2048,1280]{1,0:T(8,128)(2,1)} %all-gather.4.cloned.1.call-done), kind=kOutput, calls=%fused_computation.173 | convolution fusion | flops 403243008 | bytes 4063232 | tf_op jit(solution)/shard_map/dot_general | solution.py:169
  117.3 2.1 convolution_convert_fusion.6
  119.4 2.9 log-plus-one_add_fusion
  122.3 80.2 %while.13 = (s32[]{:T(128)}, f32[1,128,128]{2,1,0:T(8,128)S(1)}, f32[12,1,64,128]{3,2,1,0:T(8,128)}, f32[12,1,64,128]{3,2,1,0:T(8,128)}, f32[12,1,64,128]{3,2,1,...) while((s32[]{:T(128)}, f32[1,128,128]{2,1,0:T(8,128)S(1)}, ...), condition=%wide.region_3.4_spmd.clone, body=%wide.region_1.3_spmd.clone.sunk | while | flops 9003011 | bytes 5051520 | solution.py:192
  124.6 1.7 fusion.166
  126.5 1.5 fusion.168
  131.3 1.7 fusion.166
  133.2 1.5 fusion.168
  138.0 1.7 fusion.166
  139.9 1.5 fusion.168
  144.7 1.7 fusion.166
  146.5 1.5 fusion.168
  151.3 1.7 fusion.166
  153.2 1.5 fusion.168
  158.0 1.7 fusion.166
  164.7 1.7 fusion.166
  171.4 1.7 fusion.166
  173.3 1.5 fusion.168
  178.1 1.7 fusion.166
  179.9 1.5 fusion.168
  184.7 1.7 fusion.166
  186.6 1.5 fusion.168
  191.4 1.7 fusion.166
  193.3 1.5 fusion.168
  198.1 1.7 fusion.166
  205.7 2.2 fusion.68
  208.2 2.0 fusion.67
  210.2 3.1 %collective-permute-start = (bf16[30,128]{1,0:T(8,128)(2,1)S(1)}, bf16[30,128]{1,0:T(8,128)(2,1)S(1)}, u32[]{:S(2)}, u32[]{:S(2)}) collective-permute-start(bf16[30,128]{1,0:T(8,128)(2,1)S(1)} %slice.369), channel_id=1, source_target_pairs={{0,8},{8,16},{16,24},{24,32},{32,40},{40,48},{48,56},{56,64},{64,7... | collective-permute-start | bytes 23048 | tf_op jit(solution)/shard_map/ppermute | solution.py:85
  216.9 5.6 %all-to-all-start.2 = ((f32[8,1,768]{2,1,0:T(1,128)}), f32[8,1,768]{2,1,0:T(1,128)}, u32[]{:S(2)}, u32[]{:S(2)}) async-start(f32[8,1,768]{2,1,0:T(1,128)} %broadcast_in_dim.89), calls=%async_computation.2 | async-start | bytes 49152 | tf_op jit(solution)/shard_map/all_to_all | solution.py:33
  223.8 3.4 %all-to-all-done.2 = f32[8,1,768]{2,1,0:T(1,128)} async-done(((f32[8,1,768]{2,1,0:T(1,128)}), f32[8,1,768]{2,1,0:T(1,128)}, u32[]{:S(2)}, u32[]{:S(2)}) %all-to-all-start.2) | async-done | bytes 24608 | tf_op jit(solution)/shard_map/all_to_all | solution.py:33
  227.2 1.7 broadcast_in_dim.85
  228.9 7.0 %all-to-all-start.1 = ((bf16[16,129,128]{2,1,0:T(8,128)(2,1)}), bf16[16,129,128]{2,1,0:T(8,128)(2,1)}, u32[]{:S(2)}, u32[]{:S(2)}) async-start(bf16[16,129,128]{2,1,0:T(8,128)(2,1)} %broadcast_in_dim.85), calls=%async_computation.1 | async-start | bytes 1114112 | tf_op jit(solution)/shard_map/all_to_all | solution.py:33
  236.7 1.6 multiply_convert_fusion
  238.3 8.4 %all-to-all-done.1 = bf16[16,129,128]{2,1,0:T(8,128)(2,1)} async-done(((bf16[16,129,128]{2,1,0:T(8,128)(2,1)}), bf16[16,129,128]{2,1,0:T(8,128)(2,1)}, u32[]{:S(2)}, u32[]{:S(2)}) %all-to-all-start.1) | async-done | bytes 528416 | tf_op jit(solution)/shard_map/all_to_all | solution.py:33
  249.8 2.1 fusion.116
  252.0 12.5 %all_to_all.53 = bf16[8,96,256]{2,1,0:T(8,128)(2,1)S(1)} all-to-all(bf16[8,96,256]{2,1,0:T(8,128)(2,1)S(1)} %bitcast.271), channel_id=1, replica_groups=mesh['sp'=16,'tp'=8] {'tp'}, dimensions={0} | all-to-all | bytes 786432 | tf_op jit(solution)/shard_map/all_to_all | solution.py:231
  264.6 3.0 fusion.43
  267.6 3.0 fusion.40
  271.5 18.2 %all_to_all.54 = bf16[96,2,2048]{0,1,2:T(2,128)(2,1)S(1)} all-to-all(bf16[96,2,2048]{0,1,2:T(2,128)(2,1)S(1)} %copy.78), channel_id=1, replica_groups=mesh['sp'=16,'tp'=8] {'tp'}, dimensions={2} | all-to-all | bytes 1572864 | tf_op jit(solution)/shard_map/all_to_all | solution.py:239
  289.7 1.9 copy.79
  291.6 3.4 %fusion.59 = f32[768,256]{1,0:T(8,128)S(1)} fusion(bf16[768,2048]{1,0:T(8,128)(2,1)} %fusion.29, bf16[2048,1280]{1,0:T(8,128)(2,1)} %all-gather.4.cloned.1.call-done, bf16[768,2,256]{2,0,1:T(8,128)(2,1)} %bitcast.276), kind=kOutput, calls=%fused_computation.64 | convolution fusion | flops 806682624 | bytes 5373952 | tf_op jit(solution)/shard_map/dot_general | solution.py:169
  295.1 3.0 fusion.53
  (265 shorter events, 74.7 us)
Async XLA Ops:
  6.5 11.7 %copy-start = (bf16[96,2048]{1,0:T(8,128)(2,1)S(1)}, bf16[96,2048]{1,0:T(8,128)(2,1)}, u32[]{:S(2)}) copy-start(bf16[96,2048]{1,0:T(8,128)(2,1)} %param.21) | copy-start | bytes 1179652
  6.5 47.9 %all-gather.6.cloned.1.call-start = ((), (), s32[]{:S(2)}) async-start(), calls=%async_computation.6 | async-start | bytes 1114112 | tf_op jit(solution)/shard_map/all_gather | solution.py:28
  8.0 105.5 %all-gather.4.cloned.1.call-start = ((), (), s32[]{:S(2)}) async-start(), calls=%async_computation.5 | async-start | bytes 5570560 | tf_op jit(solution)/shard_map/all_gather | solution.py:28
  20.0 5.9 %copy-start.43 = (f32[128]{0:T(128)S(1)}, f32[128]{0:T(128)}, u32[]{:S(2)}) copy-start(f32[128]{0:T(128)} %param.31) | copy-start | bytes 1540
  20.0 5.9 %copy-start.13 = (f32[31,128]{1,0:T(8,128)S(1)}, f32[31,128]{1,0:T(8,128)}, u32[]{:S(2)}) copy-start(f32[31,128]{1,0:T(8,128)} %param.35) | copy-start | bytes 47620
  20.0 43.4 %all-to-all-start = ((bf16[8,96,2048]{2,1,0:T(8,128)(2,1)}), bf16[8,96,2048]{2,1,0:T(8,128)(2,1)S(1)}, u32[]{:S(2)}, u32[]{:S(2)}) async-start(bf16[8,96,2048]{2,1,0:T(8,128)(2,1)} %bitcast.267), calls=%async_computation | async-start | bytes 6291456 | tf_op jit(solution)/shard_map/all_to_all | solution.py:16
  25.9 238.7 %all-gather.8.cloned.1.call-start = ((), (), s32[]{:S(2)}) async-start(), calls=%async_computation.7 | async-start | bytes 9437184 | tf_op jit(solution)/shard_map/all_gather | solution.py:28
  55.7 8.4 %copy-start.14 = (f32[2048]{0:T(1024)S(1)}, f32[2048]{0:T(1024)}, u32[]{:S(2)}) copy-start(f32[2048]{0:T(1024)} %param.22) | copy-start | bytes 24580
  66.6 50.7 %copy-start.2 = (bf16[768,2048]{1,0:T(8,128)(2,1)S(1)}, bf16[768,2048]{1,0:T(8,128)(2,1)}, u32[]{:S(2)}) copy-start(bf16[768,2048]{1,0:T(8,128)(2,1)} %fusion.29) | copy-start | bytes 9437188
  205.7 8.2 %copy-start.5 = (f32[128,6,128]{0,2,1:T(8,128)}, f32[128,6,128]{0,2,1:T(8,128)S(1)}, u32[]{:S(2)}) copy-start(f32[128,6,128]{0,2,1:T(8,128)S(1)} %copy.72) | copy-start | bytes 1179652
  207.9 6.6 %copy-start.15 = (f32[128]{0:T(128)S(1)}, f32[128]{0:T(128)}, u32[]{:S(2)}) copy-start(f32[128]{0:T(128)} %get-tuple-element.149) | copy-start | bytes 1540
  207.9 6.6 %copy-start.16 = (f32[128]{0:T(128)S(1)}, f32[128]{0:T(128)}, u32[]{:S(2)}) copy-start(f32[128]{0:T(128)} %get-tuple-element.150) | copy-start | bytes 1540
  207.9 6.6 %copy-start.17 = (f32[128]{0:T(128)S(1)}, f32[128]{0:T(128)}, u32[]{:S(2)}) copy-start(f32[128]{0:T(128)} %get-tuple-element.151) | copy-start | bytes 1540
  207.9 6.6 %copy-start.18 = (f32[128]{0:T(128)S(1)}, f32[128]{0:T(128)}, u32[]{:S(2)}) copy-start(f32[128]{0:T(128)} %get-tuple-element.152) | copy-start | bytes 1540
  207.9 6.6 %copy-start.19 = (f32[128]{0:T(128)S(1)}, f32[128]{0:T(128)}, u32[]{:S(2)}) copy-start(f32[128]{0:T(128)} %get-tuple-element.153) | copy-start | bytes 1540
  207.9 6.6 %copy-start.20 = (f32[128]{0:T(128)S(1)}, f32[128]{0:T(128)}, u32[]{:S(2)}) copy-start(f32[128]{0:T(128)} %get-tuple-element.154) | copy-start | bytes 1540
  207.9 6.6 %copy-start.21 = (f32[128]{0:T(128)S(1)}, f32[128]{0:T(128)}, u32[]{:S(2)}) copy-start(f32[128]{0:T(128)} %get-tuple-element.155) | copy-start | bytes 1540
  208.0 6.6 %copy-start.22 = (f32[128]{0:T(128)S(1)}, f32[128]{0:T(128)}, u32[]{:S(2)}) copy-start(f32[128]{0:T(128)} %get-tuple-element.156) | copy-start | bytes 1540
  208.0 6.6 %copy-start.23 = (f32[128]{0:T(128)S(1)}, f32[128]{0:T(128)}, u32[]{:S(2)}) copy-start(f32[128]{0:T(128)} %get-tuple-element.126) | copy-start | bytes 1540
  208.0 6.6 %copy-start.24 = (f32[128]{0:T(128)S(1)}, f32[128]{0:T(128)}, u32[]{:S(2)}) copy-start(f32[128]{0:T(128)} %get-tuple-element.127) | copy-start | bytes 1540
  208.0 6.6 %copy-start.25 = (f32[128]{0:T(128)S(1)}, f32[128]{0:T(128)}, u32[]{:S(2)}) copy-start(f32[128]{0:T(128)} %get-tuple-element.128) | copy-start | bytes 1540
  208.0 6.6 %copy-start.26 = (f32[128]{0:T(128)S(1)}, f32[128]{0:T(128)}, u32[]{:S(2)}) copy-start(f32[128]{0:T(128)} %get-tuple-element.129) | copy-start | bytes 1540
  208.0 6.6 %copy-start.27 = (f32[128]{0:T(128)S(1)}, f32[128]{0:T(128)}, u32[]{:S(2)}) copy-start(f32[128]{0:T(128)} %get-tuple-element.130) | copy-start | bytes 1540
  208.0 6.6 %copy-start.28 = (f32[128]{0:T(128)S(1)}, f32[128]{0:T(128)}, u32[]{:S(2)}) copy-start(f32[128]{0:T(128)} %get-tuple-element.131) | copy-start | bytes 1540
  208.0 6.6 %copy-start.29 = (f32[128]{0:T(128)S(1)}, f32[128]{0:T(128)}, u32[]{:S(2)}) copy-start(f32[128]{0:T(128)} %get-tuple-element.132) | copy-start | bytes 1540
  208.0 6.6 %copy-start.30 = (f32[128]{0:T(128)S(1)}, f32[128]{0:T(128)}, u32[]{:S(2)}) copy-start(f32[128]{0:T(128)} %get-tuple-element.133) | copy-start | bytes 1540
  208.1 6.6 %copy-start.31 = (f32[128]{0:T(128)S(1)}, f32[128]{0:T(128)}, u32[]{:S(2)}) copy-start(f32[128]{0:T(128)} %get-tuple-element.134) | copy-start | bytes 1540
  208.1 6.6 %copy-start.32 = (f32[128]{0:T(128)S(1)}, f32[128]{0:T(128)}, u32[]{:S(2)}) copy-start(f32[128]{0:T(128)} %get-tuple-element.135) | copy-start | bytes 1540
  208.1 6.6 %copy-start.33 = (f32[128]{0:T(128)S(1)}, f32[128]{0:T(128)}, u32[]{:S(2)}) copy-start(f32[128]{0:T(128)} %get-tuple-element.136) | copy-start | bytes 1540
  208.1 6.6 %copy-start.34 = (f32[128]{0:T(128)S(1)}, f32[128]{0:T(128)}, u32[]{:S(2)}) copy-start(f32[128]{0:T(128)} %get-tuple-element.137) | copy-start | bytes 1540
  208.1 6.6 %copy-start.35 = (f32[128]{0:T(128)S(1)}, f32[128]{0:T(128)}, u32[]{:S(2)}) copy-start(f32[128]{0:T(128)} %get-tuple-element.138) | copy-start | bytes 1540
  208.1 6.6 %copy-start.36 = (f32[128]{0:T(128)S(1)}, f32[128]{0:T(128)}, u32[]{:S(2)}) copy-start(f32[128]{0:T(128)} %get-tuple-element.139) | copy-start | bytes 1540
  208.1 6.6 %copy-start.37 = (f32[128]{0:T(128)S(1)}, f32[128]{0:T(128)}, u32[]{:S(2)}) copy-start(f32[128]{0:T(128)} %get-tuple-element.140) | copy-start | bytes 1540
  208.1 6.6 %copy-start.38 = (f32[128]{0:T(128)S(1)}, f32[128]{0:T(128)}, u32[]{:S(2)}) copy-start(f32[128]{0:T(128)} %get-tuple-element.141) | copy-start | bytes 1540
  208.1 6.6 %copy-start.39 = (f32[128]{0:T(128)S(1)}, f32[128]{0:T(128)}, u32[]{:S(2)}) copy-start(f32[128]{0:T(128)} %get-tuple-element.142) | copy-start | bytes 1540
  208.1 6.6 %copy-start.40 = (f32[128]{0:T(128)S(1)}, f32[128]{0:T(128)}, u32[]{:S(2)}) copy-start(f32[128]{0:T(128)} %get-tuple-element.143) | copy-start | bytes 1540
  208.2 6.6 %copy-start.41 = (f32[128]{0:T(128)S(1)}, f32[128]{0:T(128)}, u32[]{:S(2)}) copy-start(f32[128]{0:T(128)} %get-tuple-element.144) | copy-start | bytes 1540
  210.2 4.3 %collective-permute-start = (bf16[30,128]{1,0:T(8,128)(2,1)S(1)}, bf16[30,128]{1,0:T(8,128)(2,1)S(1)}, u32[]{:S(2)}, u32[]{:S(2)}) collective-permute-start(bf16[30,128]{1,0:T(8,128)(2,1)S(1)} %slice.369), channel_id=1, source_target_pairs={{0,8},{8,16},{16,24},{24,32},{32,40},{40,48},{48,56},{56,64},{64,7... | collective-permute-start | bytes 23048 | tf_op jit(solution)/shard_map/ppermute | solution.py:85
  216.9 10.4 %all-to-all-start.2 = ((f32[8,1,768]{2,1,0:T(1,128)}), f32[8,1,768]{2,1,0:T(1,128)}, u32[]{:S(2)}, u32[]{:S(2)}) async-start(f32[8,1,768]{2,1,0:T(1,128)} %broadcast_in_dim.89), calls=%async_computation.2 | async-start | bytes 49152 | tf_op jit(solution)/shard_map/all_to_all | solution.py:33
  228.9 17.8 %all-to-all-start.1 = ((bf16[16,129,128]{2,1,0:T(8,128)(2,1)}), bf16[16,129,128]{2,1,0:T(8,128)(2,1)}, u32[]{:S(2)}, u32[]{:S(2)}) async-start(bf16[16,129,128]{2,1,0:T(8,128)(2,1)} %broadcast_in_dim.85), calls=%async_computation.1 | async-start | bytes 1114112 | tf_op jit(solution)/shard_map/all_to_all | solution.py:33
  238.3 11.1 %copy-start.6 = (f32[128,6,128]{0,2,1:T(8,128)S(1)}, f32[128,6,128]{0,2,1:T(8,128)}, u32[]{:S(2)}) copy-start(f32[128,6,128]{0,2,1:T(8,128)} %copy-done.5) | copy-start | bytes 1179652
  238.3 11.5 %copy-start.44 = (f32[128]{0:T(128)S(1)}, f32[128]{0:T(128)}, u32[]{:S(2)}) copy-start(f32[128]{0:T(128)} %param.34) | copy-start | bytes 1540
  246.7 2.6 copy-start.7
  246.7 2.6 copy-start.11
  246.7 2.7 copy-start.12
  249.8 2.1 copy-start.9
  291.6 3.4 %copy-start.3 = (bf16[768,2048]{1,0:T(8,128)(2,1)S(1)}, bf16[768,2048]{1,0:T(8,128)(2,1)}, u32[]{:S(2)}) copy-start(bf16[768,2048]{1,0:T(8,128)(2,1)} %fusion.29) | copy-start | bytes 9437188
  291.6 3.5 %copy-start.8 = (bf16[96,2,8,256]{3,0,2,1:T(8,128)(2,1)S(1)}, bf16[96,2,8,256]{3,0,2,1:T(8,128)(2,1)}, u32[]{:S(2)}) copy-start(bf16[96,2,8,256]{3,0,2,1:T(8,128)(2,1)} %copy.79) | copy-start | bytes 2359300
  (4 other events, 5.2 us)
Sparse Core Ops, SparseCore 0:
  9.4 44.9 all-gather.5
  56.6 56.9 all-gather.3
  115.3 49.7 all-gather.7
